TPU v7x, 32 devices: a whole 2x2x4 slice. The times are simulated.
32 devices in a mesh: grp: 2 (over x), ep: 16 (over z, y, core), tp: 1.
Axes of the slice: x: 2, y: 2, z: 4, core: 2. Of those that a mesh axis runs over, the one named last changes fastest.
Arguments:
- tokens: bfloat16 [2048, 1024], P(('grp', 'ep')), parts along dimension 0, may hold values from -6 to 6
- norm_gain: float32 [1024], replicated, may hold values from 0.1 to 1.9
- routes: int32 [2048, 6], P(('grp', 'ep')), parts along dimension 0, may hold values from 0 to 15, all different within a row; in each aligned block of 64 rows (0 to 63, 64 to 127, ...) at most 32 rows name the same one
- gate_weights: float32 [2048, 6], P(('grp', 'ep')), parts along dimension 0, may hold values from 0.1 to 1
- w_gate: bfloat16 [16, 1024, 2048], P('ep', None, 'tp'), may hold values from -0.1875 to 0.1875
- w_up: bfloat16 [16, 1024, 2048], P('ep', None, 'tp'), may hold values from -0.1875 to 0.1875
- w_down: bfloat16 [16, 2048, 1024], P('ep', 'tp'), may hold values from -0.125 to 0.125
Outputs:
- mixed: bfloat16 [2048, 1024], P(('grp', 'ep')), parts along dimension 0
There are 2 independent parts, one for each index of `grp`. A program takes and returns all parts, laid end to end along the dimension named above; an argument that names none is the same for every part. Nothing has to cross between parts.
Inputs may be any that keep to these rules, and one draw needn't show every extreme that they name: `routes`: each row names 6 different experts. Within the rows of one index of ep no expert is named more than 32 times, and in every draw some expert is named exactly 32 times in some index's rows.
All inputs are finite; a program needn't handle non-finite values.
Results may differ from a plain program's by a relative error of at most 0.013.
Values may be sent and summed in bfloat16 or wider, within the bound.
A program may use at most 64 MiB of HBM per device.

v0:
```python
import jax
import jax.numpy as jnp
from jax import lax
from jax.sharding import PartitionSpec as P


def hidden_rows(rows, w_gate, w_up):
    gate = jnp.dot(rows, w_gate[0], preferred_element_type=jnp.float32)
    up = jnp.dot(rows, w_up[0], preferred_element_type=jnp.float32)
    return (jax.nn.silu(gate) * up).astype(jnp.bfloat16)


def weigh_rows(combine, returned):
    upper = combine.astype(jnp.bfloat16)
    lower = (combine - upper.astype(jnp.float32)).astype(jnp.bfloat16)
    first = jnp.dot(upper, returned, preferred_element_type=jnp.float32)
    return first + jnp.dot(lower, returned, preferred_element_type=jnp.float32)


def shards(tokens, norm_gain, routes, gate_weights, w_gate, w_up, w_down):
    values = tokens.astype(jnp.float32)
    scale = lax.rsqrt(jnp.mean(values * values, axis=-1, keepdims=True) + 1e-06)
    normed = (values * scale * norm_gain).astype(jnp.bfloat16)
    width = tokens.shape[1]
    tok_dev = tokens.shape[0]
    topk = routes.shape[1]
    experts = lax.axis_size("ep")
    capacity = min(tok_dev, max(2, 4 * tok_dev * topk // (3 * experts)))
    expert_ids = jnp.arange(experts, dtype=jnp.int32)
    hits = routes[:, :, None] == expert_ids[None, None, :]
    chosen = jnp.any(hits, axis=1).astype(jnp.int32)
    weight_tok = jnp.sum(jnp.where(hits, gate_weights[:, :, None], 0.0), axis=1)
    rank = jnp.cumsum(chosen, axis=0) - chosen
    slot = jnp.where(chosen > 0, rank * experts + expert_ids[None, :], -1)
    slot_ids = jnp.arange(capacity * experts, dtype=jnp.int32)
    placed = slot[:, :, None] == slot_ids[None, None, :]
    place = jnp.any(placed, axis=1).astype(jnp.bfloat16)
    combine = jnp.sum(jnp.where(placed, weight_tok[:, :, None], 0.0), axis=1)
    dispatch = jnp.dot(place.T, normed, preferred_element_type=jnp.float32)
    dispatch = dispatch.astype(jnp.bfloat16).reshape(capacity, experts, width)
    arrived = lax.all_to_all(dispatch, "ep", split_axis=1, concat_axis=1, tiled=True)
    rows = arrived.reshape(-1, width)
    partial_value = jnp.dot(
        hidden_rows(rows, w_gate, w_up), w_down[0], preferred_element_type=jnp.float32
    )
    output = lax.psum(partial_value.astype(jnp.bfloat16), "tp")
    returned = lax.all_to_all(
        output.reshape(arrived.shape), "ep", split_axis=1, concat_axis=1, tiled=True
    )
    mixed = weigh_rows(combine, returned.reshape(-1, width))
    return mixed.astype(jnp.bfloat16)


def solution(mesh):
    in_specs = (
        P(("grp", "ep"), None),
        P(),
        P(("grp", "ep"), None),
        P(("grp", "ep"), None),
        P("ep", None, "tp"),
        P("ep", None, "tp"),
        P("ep", "tp", None),
    )
    out_specs = P(("grp", "ep"), None)
    return jax.shard_map(shards, mesh=mesh, in_specs=in_specs, out_specs=out_specs, check_vma=False)
```

profile of v0, /device:TPU:0, one launch (start us, length us, event | category | flops | bytes accessed | tf_op | source)
XLA Modules:
  0.0 82.2 jit_solution(14729144316334113847)
XLA Ops:
  0.0 0.7 fusion.23
  0.7 0.1 copy.20
  0.8 0.1 reduce_window_sum.11
  0.9 0.0 copy-start.2
  0.9 0.5 fusion.8
  1.5 1.3 %fusion.17 = f32[64]{0:T(128)S(1)} fusion(bf16[64,1024]{1,0:T(8,128)(2,1)} %param.7), kind=kLoop, calls=%fused_computation.16 | loop fusion | flops 196544 | bytes 131328 | tf_op jit(solution)/shard_map/reduce_sum | solution.py:22
  2.8 1.4 %convolution_convert_fusion = bf16[512,1024]{1,0:T(8,128)(2,1)S(1)} fusion(pred[64,512]{1,0:T(8,128)(4,1)S(1)} %fusion.8, bf16[64,1024]{1,0:T(8,128)(2,1)} %param.7, f32[1024]{0:T(1024)} %param.8, f32[64]{0:T(128)S(1)} %add_rsqrt_fusion), kind=kOutput, calls=%fused_computation.10 | convolution fusion | flops 67895296 | bytes 1216768 | tf_op jit(solution)/shard_map/dot_general | solution.py:39
  4.2 0.6 copy.22
  4.8 31.9 %all_to_all.10 = bf16[32,16,1024]{2,0,1:T(8,128)(2,1)S(1)} all-to-all(bf16[32,16,1024]{2,0,1:T(8,128)(2,1)S(1)} %copy.22), channel_id=1, replica_groups=mesh['grp'=2,'ep'=16,'tp'=1] {'ep'}, dimensions={1} | all-to-all | bytes 2097152 | tf_op jit(solution)/shard_map/all_to_all | solution.py:41
  36.7 0.6 copy.23
  37.3 0.0 copy-done.2
  37.3 4.3 %fusion.4 = f32[512,2048]{1,0:T(8,128)} fusion(bf16[512,1024]{1,0:T(8,128)(2,1)S(1)} %bitcast.29, bf16[1,1024,2048]{2,1,0:T(8,128)(2,1)S(1)} %copy-done.2), kind=kOutput, calls=%fused_computation.4 | convolution fusion | flops 2147483648 | bytes 9437184 | tf_op jit(solution)/shard_map/dot_general | solution.py:8
  41.6 9.2 %fusion.11 = bf16[512,1024]{1,0:T(8,128)(2,1)S(1)} fusion(bf16[1,2048,1024]{2,1,0:T(8,128)(2,1)} %param.13, f32[512,2048]{1,0:T(8,128)} %fusion.4, bf16[512,1024]{1,0:T(8,128)(2,1)S(1)} %bitcast.30, bf16[1,1024,2048]{2,1,0:T(8,128)(2,1)} %param.12), kind=kOutput, calls=%fused_computation.11 | convolution fusion | flops 4301783040 | bytes 14680064 | tf_op jit(solution)/shard_map/dot_general | solution.py:43
  50.8 0.0 copy-start
  50.8 0.0 copy-start.1
  50.8 1.6 %copy.24 = bf16[32,16,1024]{2,0,1:T(8,128)(2,1)} copy(bf16[32,16,1024]{2,1,0:T(8,128)(2,1)S(1)} %bitcast.31) | data formatting | bytes 2097152 | tf_op jit(solution)/shard_map/reshape | solution.py:48
  52.4 5.0 %all-to-all-start.1 = ((bf16[32,16,1024]{2,0,1:T(8,128)(2,1)}), bf16[32,16,1024]{2,0,1:T(8,128)(2,1)S(1)}, u32[]{:S(2)}, u32[]{:S(2)}) async-start(bf16[32,16,1024]{2,0,1:T(8,128)(2,1)} %copy.24), calls=%async_computation.1 | async-start | bytes 2097152 | tf_op jit(solution)/shard_map/all_to_all | solution.py:47
  57.4 0.0 copy-done
  57.5 0.0 copy-done.1
  57.5 0.1 copy.21
  57.6 0.6 select_reduce_fusion
  58.2 22.1 %all-to-all-done.1 = bf16[32,16,1024]{2,0,1:T(8,128)(2,1)S(1)} async-done(((bf16[32,16,1024]{2,0,1:T(8,128)(2,1)}), bf16[32,16,1024]{2,0,1:T(8,128)(2,1)S(1)}, u32[]{:S(2)}, u32[]{:S(2)}) %all-to-all-start.1) | async-done | bytes 1048608 | tf_op jit(solution)/shard_map/all_to_all | solution.py:47
  80.3 0.6 copy.25
  80.9 0.3 fusion.25
  81.2 1.0 %fusion.16 = bf16[64,1024]{1,0:T(8,128)(2,1)} fusion(f32[64,1024]{1,0:T(8,128)S(1)} %fusion.25, bf16[512,1024]{1,0:T(8,128)(2,1)S(1)} %bitcast.27, f32[64,512]{1,0:T(8,128)S(1)} %select_reduce_fusion), kind=kOutput, calls=%fused_computation.13 | convolution fusion | flops 67371008 | bytes 1572864 | tf_op jit(solution)/shard_map/dot_general | solution.py:17
  (4 shorter events, 0.0 us)
Async XLA Ops:
  0.9 36.4 %copy-start.2 = (bf16[1,1024,2048]{2,1,0:T(8,128)(2,1)S(1)}, bf16[1,1024,2048]{2,1,0:T(8,128)(2,1)}, u32[]{:S(2)}) copy-start(bf16[1,1024,2048]{2,1,0:T(8,128)(2,1)} %param.11) | copy-start | bytes 12582916
  50.8 6.6 %copy-start = (s32[64,6]{0,1:T(8,128)S(1)}, s32[64,6]{0,1:T(8,128)}, u32[]{:S(2)}) copy-start(s32[64,6]{0,1:T(8,128)} %param.9) | copy-start | bytes 4612
  50.8 6.6 %copy-start.1 = (f32[64,6]{0,1:T(8,128)S(1)}, f32[64,6]{0,1:T(8,128)}, u32[]{:S(2)}) copy-start(f32[64,6]{0,1:T(8,128)} %param.10) | copy-start | bytes 4612
  52.4 27.9 %all-to-all-start.1 = ((bf16[32,16,1024]{2,0,1:T(8,128)(2,1)}), bf16[32,16,1024]{2,0,1:T(8,128)(2,1)S(1)}, u32[]{:S(2)}, u32[]{:S(2)}) async-start(bf16[32,16,1024]{2,0,1:T(8,128)(2,1)} %copy.24), calls=%async_computation.1 | async-start | bytes 2097152 | tf_op jit(solution)/shard_map/all_to_all | solution.py:47
where the time goes:
time: 83.7 us; the launch traced here: 82.2 us
  blocking collectives  31.9 us (38%)
  waiting for transfers between devices  22.1 us (26%)
  matrix products  16.2 us (19%)
  starting transfers between devices  5.02 us (6%)
  local copies, waits for them, and re-layouts  3.51 us (4%)
  other arithmetic  3.31 us (4%)
    all_to_all x1, blocking collectives, shards(): lax.all_to_all(dispatch, 'ep', split_axis=1, concat_axis=1, tiled=True)  31.9 us
    all_to_all x1, waiting for transfers between devices, shards(): lax.all_to_all(output.reshape(arrived.shape), 'ep', split_axis=1, concat_...  22.1 us
    dot_general x1, matrix products, shards(): jnp.dot(hidden_rows(rows, w_gate, w_up), w_down[0], preferred_element_typ...  9.22 us
    all_to_all x1, starting transfers between devices, shards(): lax.all_to_all(output.reshape(arrived.shape), 'ep', split_axis=1, concat_...  5.02 us
    dot_general x1, matrix products, hidden_rows(): gate = jnp.dot(rows, w_gate[0], preferred_element_type=jnp.float32)  4.3 us
  transfers between devices with their start and end apart: 1, of which 1 were waited for; matrix products, arithmetic and copies ran while one was open for 1% of the time, Pallas kernels for 0%

commit v1 on v0

--- a/solution.py
+++ b/solution.py
@@ -1,6 +1,10 @@
+import functools
+
 import jax
 import jax.numpy as jnp
 from jax import lax
+from jax.experimental import pallas as pl
+from jax.experimental.pallas import tpu as pltpu
 from jax.sharding import PartitionSpec as P
 
 
@@ -51,6 +55,289 @@
     return mixed.astype(jnp.bfloat16)
 
 
+CORES = 2
+ROWS_Y = 2
+PLANE = CORES * ROWS_Y
+FF_TILE = 512
+D_TILE = 512
+
+
+def flip(index, bits):
+    bit = 1
+    while bit <= bits:
+        if bits & bit:
+            index = index + bit - 2 * bit * lax.rem(lax.div(index, bit), 2)
+        bit *= 2
+    return index
+
+
+def fused_kernel(
+    layers, cap, tok, gain, routes, weights, wg_hbm, wu_hbm, wd_hbm, out,
+    wg, wu, wd, blocks, tables, lower_tri, picked, hidden, upper_w, lower_w, parts,
+    core_in, y_out, y_in, z_out, z_in,
+    load_sem, own_send, fwd_send, core_fwd_send, block_in, tab_in,
+    core_send, core_recv, y_send, y_recv, z_send, z_recv,
+):
+    me = lax.axis_index("ep")
+    tokens, width = tok.shape
+    topk = routes.shape[1]
+    group = PLANE * tokens
+    slots = PLANE * cap
+    units = wg.shape[1]
+    z = lax.div(me, PLANE)
+    y = lax.rem(lax.div(me, CORES), ROWS_Y)
+    c = lax.rem(me, CORES)
+
+    def at(zz, yy, cc):
+        return zz * PLANE + yy * CORES + cc
+
+    oy, oc = 1 - y, 1 - c
+    partner, across = at(z, y, oc), at(z, oy, c)
+    far = [flip(z, k) for k in range(layers)]
+
+    barrier = pltpu.get_barrier_semaphore()
+    peers = [partner, across] + [at(far[k], y, c) for k in range(1, layers)]
+    for peer in peers:
+        pl.semaphore_signal(barrier, inc=1, device_id={"ep": peer})
+
+    loads = [
+        pltpu.make_async_copy(wg_hbm.at[0], wg, load_sem.at[0]),
+        pltpu.make_async_copy(wu_hbm.at[0], wu, load_sem.at[1]),
+        pltpu.make_async_copy(wd_hbm.at[0], wd, load_sem.at[2]),
+    ]
+    for load in loads:
+        load.start()
+
+    values = tok[...].astype(jnp.float32)
+    scale = lax.rsqrt(jnp.mean(values * values, axis=-1, keepdims=True) + 1e-06)
+    normed = (values * scale * gain[...]).astype(jnp.bfloat16)
+    blocks[pl.ds(pl.multiple_of(me * tokens, tokens), tokens), :] = normed
+
+    lane = lax.broadcasted_iota(jnp.int32, (tokens, 2 * tokens), 1)
+    by_expert = jnp.zeros((tokens, 2 * tokens), jnp.float32)
+    for j in range(topk):
+        by_expert = by_expert + jnp.where(routes[:, j:j + 1] == lane, weights[:, j:j + 1], 0.0)
+    doubled = jnp.concatenate([by_expert, by_expert], axis=0)
+    half = lax.broadcasted_iota(jnp.int32, doubled.shape, 0) // tokens
+    table = jnp.where(half == c, doubled, 0.0).T
+    tables[me] = table[: tables.shape[1], :]
+
+    r = lax.broadcasted_iota(jnp.int32, (group, group), 0)
+    t = lax.broadcasted_iota(jnp.int32, (group, group), 1)
+    before = (r < t) & (r // tokens == t // tokens)
+    lower_tri[...] = jnp.where(before, 1.0, 0.0).astype(jnp.bfloat16)
+
+    sent = []
+
+    def push(src, dst, send_sem, recv_sem, peer):
+        copy = pltpu.make_async_remote_copy(
+            src_ref=src, dst_ref=dst, send_sem=send_sem, recv_sem=recv_sem,
+            device_id={"ep": peer},
+        )
+        copy.start()
+        sent.append(copy)
+
+    def landed(dst, send_sem, recv_sem):
+        pltpu.make_async_remote_copy(
+            src_ref=dst, dst_ref=dst, send_sem=send_sem, recv_sem=recv_sem,
+            device_id={"ep": partner},
+        ).wait_recv()
+
+    def block(slot):
+        return blocks.at[pl.ds(pl.multiple_of(slot * tokens, tokens), tokens), :]
+
+    def share(slot, peer, sems, position):
+        push(tables.at[slot], tables.at[slot], sems.at[position, 1], tab_in.at[slot], peer)
+        push(block(slot), block(slot), sems.at[position, 0], block_in.at[slot], peer)
+
+    def await_share(slot):
+        landed(tables.at[slot], own_send.at[0, 1], tab_in.at[slot])
+        landed(block(slot), own_send.at[0, 0], block_in.at[slot])
+
+    pl.semaphore_wait(barrier, len(peers))
+    share(me, across, own_send, 0)
+    for k in range(1, layers):
+        share(me, at(far[k], y, c), own_send, k)
+    share(me, partner, core_fwd_send, 0)
+
+    def from_z(k):
+        slot = at(far[k], y, c)
+        await_share(slot)
+        share(slot, across, fwd_send, k)
+        share(slot, partner, core_fwd_send, k)
+
+    def from_y(k):
+        slot = at(far[k], oy, c)
+        await_share(slot)
+        share(slot, partner, core_fwd_send, layers + k)
+
+    def from_core(k):
+        await_share(at(far[k], y, oc))
+        await_share(at(far[k], oy, oc))
+
+    def gather(k):
+        base = far[k] * PLANE
+        pairs = [
+            tables[base + CORES * yy, pl.ds(me, 1), :] + tables[base + CORES * yy + 1, pl.ds(me, 1), :]
+            for yy in range(ROWS_Y)
+        ]
+        weight = jnp.broadcast_to(jnp.concatenate(pairs, axis=1), (slots, group))
+        chosen = weight > 0.0
+        rank = jnp.dot(
+            jnp.where(chosen, 1.0, 0.0).astype(jnp.bfloat16), lower_tri[...],
+            preferred_element_type=jnp.float32,
+        )
+        row = lax.broadcasted_iota(jnp.int32, (slots, group), 0)
+        column = lax.broadcasted_iota(jnp.int32, (slots, group), 1)
+        place = chosen & (rank == (row % cap).astype(jnp.float32)) & (row // cap == column // tokens)
+        pick = jnp.where(place, 1.0, 0.0).astype(jnp.bfloat16)
+        spread = jnp.where(place, weight, 0.0).T
+        upper = spread.astype(jnp.bfloat16)
+        upper_w[...] = upper
+        lower_w[...] = (spread - upper.astype(jnp.float32)).astype(jnp.bfloat16)
+        rows = blocks[pl.ds(pl.multiple_of(base * tokens, group), group), :]
+        picked[...] = jnp.dot(pick, rows, preferred_element_type=jnp.float32).astype(jnp.bfloat16)
+
+    def gate_up():
+        @pl.loop(0, units // FF_TILE)
+        def _(i):
+            cols = pl.ds(pl.multiple_of(i * FF_TILE, FF_TILE), FF_TILE)
+            gate = jnp.dot(picked[...], wg[:, cols], preferred_element_type=jnp.float32)
+            up = jnp.dot(picked[...], wu[:, cols], preferred_element_type=jnp.float32)
+            hidden[:, cols] = (gate / (1.0 + jnp.exp(-gate)) * up).astype(jnp.bfloat16)
+
+    def down(k):
+        @pl.loop(0, width // D_TILE)
+        def _(i):
+            cols = pl.ds(pl.multiple_of(i * D_TILE, D_TILE), D_TILE)
+            expert_out = jnp.dot(
+                hidden[...], wd[:, cols], preferred_element_type=jnp.float32
+            ).astype(jnp.bfloat16)
+            part = jnp.dot(upper_w[...], expert_out, preferred_element_type=jnp.float32)
+            part = part + jnp.dot(lower_w[...], expert_out, preferred_element_type=jnp.float32)
+            parts[k, :, cols] = part.astype(jnp.bfloat16)
+
+    def part_of(k, yy, cc):
+        start = pl.multiple_of((yy * CORES + cc) * tokens, tokens)
+        return parts.at[k, pl.ds(start, tokens), :]
+
+    def core_stage(k):
+        for position, yy in enumerate((oy, y)):
+            push(part_of(k, yy, oc), core_in.at[k, position],
+                 core_send.at[k, position], core_recv.at[k, position], partner)
+
+    def y_stage(k):
+        landed(core_in.at[k, 0], core_send.at[k, 0], core_recv.at[k, 0])
+        both = part_of(k, oy, c)[...].astype(jnp.float32) + core_in[k, 0].astype(jnp.float32)
+        y_out[k] = both.astype(jnp.bfloat16)
+        push(y_out.at[k], y_in.at[k], y_send.at[k], y_recv.at[k], across)
+
+    def layer_sum(k):
+        landed(core_in.at[k, 1], core_send.at[k, 1], core_recv.at[k, 1])
+        both = part_of(k, y, c)[...].astype(jnp.float32) + core_in[k, 1].astype(jnp.float32)
+        landed(y_in.at[k], y_send.at[k], y_recv.at[k])
+        return both + y_in[k].astype(jnp.float32)
+
+    def z_stage(k):
+        if k == 0:
+            return
+        z_out[k] = layer_sum(k).astype(jnp.bfloat16)
+        push(z_out.at[k], z_in.at[k], z_send.at[k], z_recv.at[k], at(far[k], y, c))
+
+    for k in range(layers):
+        from_y(k)
+        from_core(k)
+        gather(k)
+        if k == 0:
+            loads[0].wait()
+            loads[1].wait()
+        gate_up()
+        if k + 1 < layers:
+            from_z(k + 1)
+        if k >= 2:
+            z_stage(k - 2)
+        if k >= 1:
+            y_stage(k - 1)
+        if k == 0:
+            loads[2].wait()
+        down(k)
+        core_stage(k)
+    if layers >= 2:
+        z_stage(layers - 2)
+    y_stage(layers - 1)
+    total = layer_sum(0)
+    z_stage(layers - 1)
+    for k in range(1, layers):
+        landed(z_in.at[k], z_send.at[k], z_recv.at[k])
+        total = total + z_in[k].astype(jnp.float32)
+    out[...] = total.astype(jnp.bfloat16)
+    for copy in sent:
+        copy.wait_send()
+
+
+def fused_shards(tokens, norm_gain, routes, gate_weights, w_gate, w_up, w_down):
+    tok_dev, width = tokens.shape
+    units = w_gate.shape[2]
+    topk = routes.shape[1]
+    experts = lax.axis_size("ep")
+    layers = experts // PLANE
+    cap = min(tok_dev, max(2, 4 * tok_dev * topk // (3 * experts)))
+    vmem = pl.BlockSpec(memory_space=pltpu.VMEM)
+    hbm = pl.BlockSpec(memory_space=pltpu.MemorySpace.HBM)
+    dma = pltpu.SemaphoreType.DMA
+    bf = jnp.bfloat16
+    return pl.pallas_call(
+        functools.partial(fused_kernel, layers, cap),
+        out_shape=jax.ShapeDtypeStruct((tok_dev, width), bf),
+        in_specs=[vmem] * 4 + [hbm] * 3,
+        out_specs=vmem,
+        scratch_shapes=[
+            pltpu.VMEM((width, units), bf),
+            pltpu.VMEM((width, units), bf),
+            pltpu.VMEM((units, width), bf),
+            pltpu.VMEM((experts * tok_dev, width), bf),
+            pltpu.VMEM((experts, experts, 2 * tok_dev), jnp.float32),
+            pltpu.VMEM((PLANE * tok_dev, PLANE * tok_dev), bf),
+            pltpu.VMEM((PLANE * cap, width), bf),
+            pltpu.VMEM((PLANE * cap, units), bf),
+            pltpu.VMEM((PLANE * tok_dev, PLANE * cap), bf),
+            pltpu.VMEM((PLANE * tok_dev, PLANE * cap), bf),
+            pltpu.VMEM((layers, PLANE * tok_dev, width), bf),
+            pltpu.VMEM((layers, 2, tok_dev, width), bf),
+            pltpu.VMEM((layers, tok_dev, width), bf),
+            pltpu.VMEM((layers, tok_dev, width), bf),
+            pltpu.VMEM((layers, tok_dev, width), bf),
+            pltpu.VMEM((layers, tok_dev, width), bf),
+            dma((3,)),
+            dma((layers, 2)),
+            dma((layers, 2)),
+            dma((2 * layers, 2)),
+            dma((experts,)),
+            dma((experts,)),
+            dma((layers, 2)),
+            dma((layers, 2)),
+            dma((layers,)),
+            dma((layers,)),
+            dma((layers,)),
+            dma((layers,)),
+        ],
+        compiler_params=pltpu.CompilerParams(
+            collective_id=0, has_side_effects=True, vmem_limit_bytes=48 * 1024 * 1024
+        ),
+    )(tokens, norm_gain.reshape(1, width), routes, gate_weights, w_gate, w_up, w_down)
+
+
+def fits_fused(mesh, tokens, w_gate):
+    experts = mesh.shape["ep"]
+    layers = experts // PLANE
+    tok_dev = tokens.shape[0] // (mesh.shape["grp"] * experts)
+    return (
+        mesh.shape["tp"] == 1 and experts % PLANE == 0 and layers & (layers - 1) == 0
+        and tok_dev == 64 and experts % 8 == 0 and experts <= 128
+        and tokens.shape[1] % D_TILE == 0 and w_gate.shape[2] % FF_TILE == 0
+    )
+
+
 def solution(mesh):
     in_specs = (
         P(("grp", "ep"), None),
@@ -62,4 +349,11 @@
         P("ep", "tp", None),
     )
     out_specs = P(("grp", "ep"), None)
-    return jax.shard_map(shards, mesh=mesh, in_specs=in_specs, out_specs=out_specs, check_vma=False)
+
+    def layer(tokens, norm_gain, routes, gate_weights, w_gate, w_up, w_down):
+        body = fused_shards if fits_fused(mesh, tokens, w_gate) else shards
+        return jax.shard_map(
+            body, mesh=mesh, in_specs=in_specs, out_specs=out_specs, check_vma=False
+        )(tokens, norm_gain, routes, gate_weights, w_gate, w_up, w_down)
+
+    return layer

time: 83.7 us -> 58.7 us (0.70); the launches traced: 82.2 us -> 58.5 us
  Pallas kernels: 0 us -> 52.5 us
  blocking collectives: 31.9 us -> 0 us
  waiting for transfers between devices: 22.1 us -> 0 us
  matrix products: 16.2 us -> 0 us
  starting transfers between devices: 5.02 us -> 0 us
  other arithmetic: 3.31 us -> 0 us
  local copies, waits for them, and re-layouts: 3.51 us -> 5.99 us
    pallas_call x0 -> x1, Pallas kernels: none -> 52.5 us  [fused_shards(): pl.pallas_call(functools.partial(fused_kernel, layers, cap), out_shape=ja...]
    all_to_all x1 -> x0, blocking collectives: 31.9 us -> none  [shards(): lax.all_to_all(dispatch, 'ep', split_axis=1, concat_axis=1, tiled=True)]
    all_to_all x1 -> x0, waiting for transfers between devices: 22.1 us -> none  [shards(): lax.all_to_all(output.reshape(arrived.shape), 'ep', split_axis=1, concat_...]
    dot_general x5 -> x0, matrix products: 16.2 us -> none  [the longest x1 9.22 us: shards(): jnp.dot(hidden_rows(rows, w_gate, w_up), w_down[0], preferred_element_typ...]
    unnamed x6 -> x9, local copies, waits for them, and re-layouts: 0.02 us -> 5.99 us
    all_to_all x1 -> x0, starting transfers between devices: 5.02 us -> none  [shards(): lax.all_to_all(output.reshape(arrived.shape), 'ep', split_axis=1, concat_...]
    reshape x2 -> x0, local copies, waits for them, and re-layouts: 2.15 us -> none  [the longest x1 1.57 us: shards(): output.reshape(arrived.shape)]
    reduce_sum x3 -> x0, other arithmetic: 1.96 us -> none  [the longest x1 1.31 us: shards(): scale = lax.rsqrt(jnp.mean(values * values, axis=-1, keepdims=True) + 1e-06)]
  transfers between devices with their start and end apart: 1 -> 0, of which waited for: 1 -> 0; matrix products, arithmetic and copies ran while one was open for 1% -> 0% of each run, Pallas kernels for 0% -> 0%
where the time goes in v1:
time: 58.7 us; the launch traced here: 58.5 us
  Pallas kernels  52.5 us (89%)
  local copies, waits for them, and re-layouts  5.99 us (10%)
    pallas_call x1, Pallas kernels, fused_shards(): pl.pallas_call(functools.partial(fused_kernel, layers, cap), out_shape=ja...  52.5 us
    unnamed x9, local copies, waits for them, and re-layouts  5.99 us

profile of v1, /device:TPU:0, one launch (start us, length us, event | category | flops | bytes accessed | tf_op | source)
XLA Modules:
  0.0 58.5 jit_solution(9501688619338021264)
XLA Ops:
  0.0 0.8 %copy.8.routes = s32[64,6]{1,0:T(8,128)S(1)} copy(s32[64,6]{0,1:T(8,128)} %param.9) | data formatting | bytes 3072 | tf_op args[2]
  0.8 0.8 %copy.9.weights = f32[64,6]{1,0:T(8,128)S(1)} copy(f32[64,6]{0,1:T(8,128)} %param.10) | data formatting | bytes 3072 | tf_op args[3]
  1.6 0.0 copy-start
  1.6 2.2 %copy-done = bf16[1,1024,2048]{2,1,0:T(8,128)(2,1)S(1)} copy-done((bf16[1,1024,2048]{2,1,0:T(8,128)(2,1)S(1)}, bf16[1,1024,2048]{2,1,0:T(8,128)(2,1)}, u32[]{:S(2)}) %copy-start) | copy-done | bytes 4194328
  3.7 0.0 copy-start.1
  3.7 0.9 %copy-done.1 = bf16[64,1024]{1,0:T(8,128)(2,1)S(1)} copy-done((bf16[64,1024]{1,0:T(8,128)(2,1)S(1)}, bf16[64,1024]{1,0:T(8,128)(2,1)}, u32[]{:S(2)}) %copy-start.1) | copy-done | bytes 131096
  4.6 0.0 copy-start.2
  4.6 0.7 %copy-done.2 = f32[1024]{0:T(1024)S(1)} copy-done((f32[1024]{0:T(1024)S(1)}, f32[1024]{0:T(1024)}, u32[]{:S(2)}) %copy-start.2) | copy-done | bytes 4120
  5.3 52.5 %shard_map.73 = bf16[64,1024]{1,0:T(8,128)(2,1)S(1)} custom-call(bf16[64,1024]{1,0:T(8,128)(2,1)S(1)} %copy-done.1, f32[1,1024]{1,0:T(1,128)S(1)} %bitcast.1, s32[64,6]{1,0:T(8,128)S(1)} %copy.8.routes, f32[64,6]{1,0:T(8,128)S(1)} %copy.9.weights, bf16[1,1024,2048]{2,1,0:T(8,128)(2,1)S(1)} %copy-done, bf16[1,1024,2048]{2,1,0:T(8,128)(2,1)} %wu_hbm.1, ...), custom_call_target="tpu_custom_call" | custom-call | tf_op jit(solution)/shard_map/pallas_call | solution.py:289
  57.8 0.7 %copy.11 = bf16[64,1024]{1,0:T(8,128)(2,1)} copy(bf16[64,1024]{1,0:T(8,128)(2,1)S(1)} %shard_map.73) | data formatting | bytes 262144
Async XLA Ops:
  1.6 2.2 %copy-start = (bf16[1,1024,2048]{2,1,0:T(8,128)(2,1)S(1)}, bf16[1,1024,2048]{2,1,0:T(8,128)(2,1)}, u32[]{:S(2)}) copy-start(bf16[1,1024,2048]{2,1,0:T(8,128)(2,1)} %wg_hbm.1) | copy-start | bytes 12582916
  3.7 0.9 %copy-start.1 = (bf16[64,1024]{1,0:T(8,128)(2,1)S(1)}, bf16[64,1024]{1,0:T(8,128)(2,1)}, u32[]{:S(2)}) copy-start(bf16[64,1024]{1,0:T(8,128)(2,1)} %tok.1) | copy-start | bytes 393220
  4.6 0.7 %copy-start.2 = (f32[1024]{0:T(1024)S(1)}, f32[1024]{0:T(1024)}, u32[]{:S(2)}) copy-start(f32[1024]{0:T(1024)} %param.8) | copy-start | bytes 12292

commit v2 on v1

v2 whole, which is shorter than its diff:
```python
import functools

import jax
import jax.numpy as jnp
from jax import lax
from jax.experimental import pallas as pl
from jax.experimental.pallas import tpu as pltpu
from jax.sharding import PartitionSpec as P


def hidden_rows(rows, w_gate, w_up):
    gate = jnp.dot(rows, w_gate[0], preferred_element_type=jnp.float32)
    up = jnp.dot(rows, w_up[0], preferred_element_type=jnp.float32)
    return (jax.nn.silu(gate) * up).astype(jnp.bfloat16)


def weigh_rows(combine, returned):
    upper = combine.astype(jnp.bfloat16)
    lower = (combine - upper.astype(jnp.float32)).astype(jnp.bfloat16)
    first = jnp.dot(upper, returned, preferred_element_type=jnp.float32)
    return first + jnp.dot(lower, returned, preferred_element_type=jnp.float32)


def shards(tokens, norm_gain, routes, gate_weights, w_gate, w_up, w_down):
    values = tokens.astype(jnp.float32)
    scale = lax.rsqrt(jnp.mean(values * values, axis=-1, keepdims=True) + 1e-06)
    normed = (values * scale * norm_gain).astype(jnp.bfloat16)
    width = tokens.shape[1]
    tok_dev = tokens.shape[0]
    topk = routes.shape[1]
    experts = lax.axis_size("ep")
    capacity = min(tok_dev, max(2, 4 * tok_dev * topk // (3 * experts)))
    expert_ids = jnp.arange(experts, dtype=jnp.int32)
    hits = routes[:, :, None] == expert_ids[None, None, :]
    chosen = jnp.any(hits, axis=1).astype(jnp.int32)
    weight_tok = jnp.sum(jnp.where(hits, gate_weights[:, :, None], 0.0), axis=1)
    rank = jnp.cumsum(chosen, axis=0) - chosen
    slot = jnp.where(chosen > 0, rank * experts + expert_ids[None, :], -1)
    slot_ids = jnp.arange(capacity * experts, dtype=jnp.int32)
    placed = slot[:, :, None] == slot_ids[None, None, :]
    place = jnp.any(placed, axis=1).astype(jnp.bfloat16)
    combine = jnp.sum(jnp.where(placed, weight_tok[:, :, None], 0.0), axis=1)
    dispatch = jnp.dot(place.T, normed, preferred_element_type=jnp.float32)
    dispatch = dispatch.astype(jnp.bfloat16).reshape(capacity, experts, width)
    arrived = lax.all_to_all(dispatch, "ep", split_axis=1, concat_axis=1, tiled=True)
    rows = arrived.reshape(-1, width)
    partial_value = jnp.dot(
        hidden_rows(rows, w_gate, w_up), w_down[0], preferred_element_type=jnp.float32
    )
    output = lax.psum(partial_value.astype(jnp.bfloat16), "tp")
    returned = lax.all_to_all(
        output.reshape(arrived.shape), "ep", split_axis=1, concat_axis=1, tiled=True
    )
    mixed = weigh_rows(combine, returned.reshape(-1, width))
    return mixed.astype(jnp.bfloat16)


CORES = 2
ROWS_Y = 2
PLANE = CORES * ROWS_Y
FF_TILE = 512
HALVES = 2


def near_first(index, layers):
    orders = [sorted(range(layers), key=lambda v: (abs(v - own), v)) for own in range(layers)]
    result = []
    for k in range(layers):
        value = orders[0][k]
        for own in range(1, layers):
            value = jnp.where(index == own, orders[own][k], value)
        result.append(value)
    return result


def fused_kernel(
    layers, cap, tok_hbm, gain_hbm, routes_hbm, weights_hbm, wg_hbm, wu_hbm, wd_hbm, out,
    tok, gain, routes, weights, wg, wu, wd, blocks, tables, lower_tri, picked, hidden,
    upper_w, lower_w, parts, core_in, y_out, y_in, z_out, z_in,
    load_sem, own_send, line_send, fwd_send, core_fwd_send, tab_send, block_in, tab_in,
    core_send, core_recv, y_send, y_recv, z_send, z_recv,
):
    me = lax.axis_index("ep")
    tokens, width = tok.shape
    topk = routes.shape[0]
    group = PLANE * tokens
    slots = PLANE * cap
    units = wg.shape[1]
    span = width // HALVES
    experts = tables.shape[0]
    z = lax.div(me, PLANE)
    y = lax.rem(lax.div(me, CORES), ROWS_Y)
    c = lax.rem(me, CORES)

    def at(zz, yy, cc):
        return zz * PLANE + yy * CORES + cc

    oy, oc = 1 - y, 1 - c
    partner, across = at(z, y, oc), at(z, oy, c)
    far = near_first(z, layers)

    barrier = pltpu.get_barrier_semaphore()
    peers = [partner, across] + [at(far[k], y, c) for k in range(1, layers)]
    for peer in peers:
        pl.semaphore_signal(barrier, inc=1, device_id={"ep": peer})

    small = [
        pltpu.make_async_copy(tok_hbm, tok, load_sem.at[3]),
        pltpu.make_async_copy(gain_hbm, gain, load_sem.at[4]),
        pltpu.make_async_copy(routes_hbm, routes, load_sem.at[5]),
        pltpu.make_async_copy(weights_hbm, weights, load_sem.at[6]),
    ]
    loads = [
        pltpu.make_async_copy(wg_hbm.at[0], wg, load_sem.at[0]),
        pltpu.make_async_copy(wu_hbm.at[0], wu, load_sem.at[1]),
        pltpu.make_async_copy(wd_hbm.at[0], wd, load_sem.at[2]),
    ]
    for load in small + loads:
        load.start()

    r = lax.broadcasted_iota(jnp.int32, (group, group), 0)
    t = lax.broadcasted_iota(jnp.int32, (group, group), 1)
    before = (r < t) & (r // tokens == t // tokens)
    lower_tri[...] = jnp.where(before, 1.0, 0.0).astype(jnp.bfloat16)

    for load in small:
        load.wait()
    values = tok[...].astype(jnp.float32)
    scale = lax.rsqrt(jnp.mean(values * values, axis=-1, keepdims=True) + 1e-06)
    normed = (values * scale * gain[...]).astype(jnp.bfloat16)
    own_rows = pl.ds(pl.multiple_of(me * tokens, tokens), tokens)
    for h in range(HALVES):
        blocks[h, own_rows, :] = normed[:, h * span:(h + 1) * span]

    expert_id = lax.broadcasted_iota(jnp.int32, (experts, tokens), 0)
    table = jnp.zeros((experts, tokens), jnp.float32)
    for j in range(topk):
        table = table + jnp.where(routes[j:j + 1, :] == expert_id, weights[j:j + 1, :], 0.0)
    doubled = jnp.concatenate([table, table], axis=1)
    half = lax.broadcasted_iota(jnp.int32, doubled.shape, 1) // tokens
    tables[me] = jnp.where(half == c, doubled, 0.0)

    sent = []

    def push(src, dst, send_sem, recv_sem, peer, when=None):
        copy = pltpu.make_async_remote_copy(
            src_ref=src, dst_ref=dst, send_sem=send_sem, recv_sem=recv_sem,
            device_id={"ep": peer},
        )
        if when is None:
            copy.start()
        else:
            pl.when(when)(copy.start)
        sent.append((copy, when))

    def landed(dst, send_sem, recv_sem):
        pltpu.make_async_remote_copy(
            src_ref=dst, dst_ref=dst, send_sem=send_sem, recv_sem=recv_sem,
            device_id={"ep": partner},
        ).wait_recv()

    def block(h, slot):
        return blocks.at[h, pl.ds(pl.multiple_of(slot * tokens, tokens), tokens), :]

    counter = [0]

    def share(h, slot, peer, sem, when=None):
        if h == 0:
            position = counter[0]
            counter[0] += 1
            push(tables.at[slot], tables.at[slot], tab_send.at[position], tab_in.at[slot], peer, when)
        push(block(h, slot), block(h, slot), sem, block_in.at[slot, h], peer, when)

    def await_share(h, slot):
        if h == 0:
            landed(tables.at[slot], tab_send.at[0], tab_in.at[slot])
        landed(block(h, slot), own_send.at[0, h], block_in.at[slot, h])

    pl.semaphore_wait(barrier, len(peers))
    for h in range(HALVES):
        share(h, me, across, own_send.at[0, h])
        share(h, me, at(lax.rem(z + 1, layers), y, c), own_send.at[1, h], z + 1 < layers)
        share(h, me, at(lax.rem(z + layers - 1, layers), y, c), own_send.at[2, h], z > 0)
    for h in range(HALVES):
        share(h, me, partner, core_fwd_send.at[0, h])

    def from_z(k):
        slot = at(far[k], y, c)
        step = jnp.where(far[k] < z, 1, -1)
        inside = (z + step >= 0) & (z + step < layers)
        onward = at(lax.rem(z + step + layers, layers), y, c)
        for h in range(HALVES):
            await_share(h, slot)
            share(h, slot, onward, line_send.at[k, h], inside)
            share(h, slot, across, fwd_send.at[k, h])
            share(h, slot, partner, core_fwd_send.at[k, h])

    def from_y(k):
        slot = at(far[k], oy, c)
        for h in range(HALVES):
            await_share(h, slot)
            share(h, slot, partner, core_fwd_send.at[layers + k, h])

    def from_core(k):
        for h in range(HALVES):
            await_share(h, at(far[k], y, oc))
            await_share(h, at(far[k], oy, oc))

    def gather(k):
        base = far[k] * PLANE
        pairs = [
            tables[base + CORES * yy, pl.ds(me, 1), :] + tables[base + CORES * yy + 1, pl.ds(me, 1), :]
            for yy in range(ROWS_Y)
        ]
        weight = jnp.broadcast_to(jnp.concatenate(pairs, axis=1), (slots, group))
        chosen = weight > 0.0
        rank = jnp.dot(
            jnp.where(chosen, 1.0, 0.0).astype(jnp.bfloat16), lower_tri[...],
            preferred_element_type=jnp.float32,
        )
        row = lax.broadcasted_iota(jnp.int32, (slots, group), 0)
        column = lax.broadcasted_iota(jnp.int32, (slots, group), 1)
        place = chosen & (rank == (row % cap).astype(jnp.float32)) & (row // cap == column // tokens)
        pick = jnp.where(place, 1.0, 0.0).astype(jnp.bfloat16)
        spread = jnp.where(place, weight, 0.0).T
        upper = spread.astype(jnp.bfloat16)
        upper_w[...] = upper
        lower_w[...] = (spread - upper.astype(jnp.float32)).astype(jnp.bfloat16)
        for h in range(HALVES):
            rows = blocks[h, pl.ds(pl.multiple_of(base * tokens, group), group), :]
            found = jnp.dot(pick, rows, preferred_element_type=jnp.float32)
            picked[:, h * span:(h + 1) * span] = found.astype(jnp.bfloat16)

    def gate_up():
        @pl.loop(0, units // FF_TILE)
        def _(i):
            cols = pl.ds(pl.multiple_of(i * FF_TILE, FF_TILE), FF_TILE)
            gate = jnp.dot(picked[...], wg[:, cols], preferred_element_type=jnp.float32)
            up = jnp.dot(picked[...], wu[:, cols], preferred_element_type=jnp.float32)
            hidden[:, cols] = (gate / (1.0 + jnp.exp(-gate)) * up).astype(jnp.bfloat16)

    def part_of(k, h, yy, cc):
        start = pl.multiple_of((yy * CORES + cc) * tokens, tokens)
        return parts.at[k, h, pl.ds(start, tokens), :]

    def down(k):
        for h in range(HALVES):
            expert_out = jnp.dot(
                hidden[...], wd[:, h * span:(h + 1) * span], preferred_element_type=jnp.float32
            ).astype(jnp.bfloat16)
            part = jnp.dot(upper_w[...], expert_out, preferred_element_type=jnp.float32)
            part = part + jnp.dot(lower_w[...], expert_out, preferred_element_type=jnp.float32)
            parts[k, h] = part.astype(jnp.bfloat16)
            for position, yy in enumerate((oy, y)):
                push(part_of(k, h, yy, oc), core_in.at[k, h, position],
                     core_send.at[k, h, position], core_recv.at[k, h, position], partner)

    def y_stage(k):
        for h in range(HALVES):
            landed(core_in.at[k, h, 0], core_send.at[k, h, 0], core_recv.at[k, h, 0])
            both = part_of(k, h, oy, c)[...].astype(jnp.float32) + core_in[k, h, 0].astype(jnp.float32)
            y_out[k, h] = both.astype(jnp.bfloat16)
            push(y_out.at[k, h], y_in.at[k, h], y_send.at[k, h], y_recv.at[k, h], across)

    def layer_sum(k, h):
        landed(core_in.at[k, h, 1], core_send.at[k, h, 1], core_recv.at[k, h, 1])
        both = part_of(k, h, y, c)[...].astype(jnp.float32) + core_in[k, h, 1].astype(jnp.float32)
        landed(y_in.at[k, h], y_send.at[k, h], y_recv.at[k, h])
        return both + y_in[k, h].astype(jnp.float32)

    def z_stage(k):
        for h in range(HALVES):
            z_out[k, h] = layer_sum(k, h).astype(jnp.bfloat16)
            push(z_out.at[k, h], z_in.at[z, h], z_send.at[k, h], z_recv.at[z, h], at(far[k], y, c))

    last = layers - 1
    if last >= 1:
        from_z(1)
    for k in range(layers):
        from_y(k)
        if k == 1:
            for ahead in range(3, layers):
                from_z(ahead)
        from_core(k)
        gather(k)
        if k == 0:
            loads[0].wait()
            loads[1].wait()
        gate_up()
        if k == 0:
            if last >= 2:
                from_z(2)
            loads[2].wait()
        if k >= 3:
            z_stage(k - 2)
        if k >= 1:
            y_stage(k - 1)
        down(k)
    if last >= 2:
        z_stage(last - 1)
    y_stage(last)
    totals = [layer_sum(0, h) for h in range(HALVES)]
    if last >= 1:
        z_stage(last)
    for h in range(HALVES):
        total = totals[h]
        for k in range(1, layers):
            landed(z_in.at[far[k], h], z_send.at[k, h], z_recv.at[far[k], h])
            total = total + z_in[far[k], h].astype(jnp.float32)
        out[:, h * span:(h + 1) * span] = total.astype(jnp.bfloat16)
    for copy, when in sent:
        if when is None:
            copy.wait_send()
        else:
            pl.when(when)(copy.wait_send)


def fused_shards(tokens, norm_gain, routes, gate_weights, w_gate, w_up, w_down):
    tok_dev, width = tokens.shape
    units = w_gate.shape[2]
    topk = routes.shape[1]
    experts = lax.axis_size("ep")
    layers = experts // PLANE
    cap = min(tok_dev, max(2, 4 * tok_dev * topk // (3 * experts)))
    vmem = pl.BlockSpec(memory_space=pltpu.VMEM)
    hbm = pl.BlockSpec(memory_space=pltpu.MemorySpace.HBM)
    dma = pltpu.SemaphoreType.DMA
    bf = jnp.bfloat16
    span = width // HALVES
    return pl.pallas_call(
        functools.partial(fused_kernel, layers, cap),
        out_shape=jax.ShapeDtypeStruct((tok_dev, width), bf),
        in_specs=[hbm] * 7,
        out_specs=vmem,
        scratch_shapes=[
            pltpu.VMEM((tok_dev, width), bf),
            pltpu.VMEM((1, width), jnp.float32),
            pltpu.VMEM((topk, tok_dev), jnp.int32),
            pltpu.VMEM((topk, tok_dev), jnp.float32),
            pltpu.VMEM((width, units), bf),
            pltpu.VMEM((width, units), bf),
            pltpu.VMEM((units, width), bf),
            pltpu.VMEM((HALVES, experts * tok_dev, span), bf),
            pltpu.VMEM((experts, experts, 2 * tok_dev), jnp.float32),
            pltpu.VMEM((PLANE * tok_dev, PLANE * tok_dev), bf),
            pltpu.VMEM((PLANE * cap, width), bf),
            pltpu.VMEM((PLANE * cap, units), bf),
            pltpu.VMEM((PLANE * tok_dev, PLANE * cap), bf),
            pltpu.VMEM((PLANE * tok_dev, PLANE * cap), bf),
            pltpu.VMEM((layers, HALVES, PLANE * tok_dev, span), bf),
            pltpu.VMEM((layers, HALVES, 2, tok_dev, span), bf),
            pltpu.VMEM((layers, HALVES, tok_dev, span), bf),
            pltpu.VMEM((layers, HALVES, tok_dev, span), bf),
            pltpu.VMEM((layers, HALVES, tok_dev, span), bf),
            pltpu.VMEM((layers, HALVES, tok_dev, span), bf),
            dma((7,)),
            dma((3, HALVES)),
            dma((layers, HALVES)),
            dma((layers, HALVES)),
            dma((2 * layers, HALVES)),
            dma((5 * layers,)),
            dma((experts, HALVES)),
            dma((experts,)),
            dma((layers, HALVES, 2)),
            dma((layers, HALVES, 2)),
            dma((layers, HALVES)),
            dma((layers, HALVES)),
            dma((layers, HALVES)),
            dma((layers, HALVES)),
        ],
        compiler_params=pltpu.CompilerParams(
            collective_id=0, has_side_effects=True, vmem_limit_bytes=60 * 1024 * 1024
        ),
    )(tokens, norm_gain.reshape(1, width), routes.T, gate_weights.T, w_gate, w_up, w_down)


def fits_fused(mesh, tokens, w_gate):
    experts = mesh.shape["ep"]
    layers = experts // PLANE
    tok_dev = tokens.shape[0] // (mesh.shape["grp"] * experts)
    return (
        mesh.shape["tp"] == 1 and experts % PLANE == 0 and layers & (layers - 1) == 0
        and tok_dev == 64 and experts % 8 == 0 and experts <= 128
        and tokens.shape[1] % (128 * HALVES) == 0 and w_gate.shape[2] % FF_TILE == 0
    )


def solution(mesh):
    in_specs = (
        P(("grp", "ep"), None),
        P(),
        P(("grp", "ep"), None),
        P(("grp", "ep"), None),
        P("ep", None, "tp"),
        P("ep", None, "tp"),
        P("ep", "tp", None),
    )
    out_specs = P(("grp", "ep"), None)

    def layer(tokens, norm_gain, routes, gate_weights, w_gate, w_up, w_down):
        body = fused_shards if fits_fused(mesh, tokens, w_gate) else shards
        return jax.shard_map(
            body, mesh=mesh, in_specs=in_specs, out_specs=out_specs, check_vma=False
        )(tokens, norm_gain, routes, gate_weights, w_gate, w_up, w_down)

    return layer
```

time: 58.7 us -> 48.7 us (0.83)
  Pallas kernels: 52.5 us -> 47 us
  local copies, waits for them, and re-layouts: 5.99 us -> 1.57 us
    pallas_call x1, Pallas kernels: 52.5 us -> 47 us  [fused_shards(): pl.pallas_call(functools.partial(fused_kernel, layers, cap), out_shape=ja...]
    unnamed x9 -> x1, local copies, waits for them, and re-layouts: 5.99 us -> 1.57 us
where the time goes in v2:
time: 48.7 us; the launch traced here: 48.6 us
  Pallas kernels  47 us (97%)
  local copies, waits for them, and re-layouts  1.57 us (3%)
    pallas_call x1, Pallas kernels, fused_shards(): pl.pallas_call(functools.partial(fused_kernel, layers, cap), out_shape=ja...  47 us
    unnamed x1, local copies, waits for them, and re-layouts  1.57 us

profile of v2, /device:TPU:0, one launch (start us, length us, event | category | flops | bytes accessed | tf_op | source)
XLA Modules:
  0.0 48.6 jit_solution(16998214138441350840)
XLA Ops:
  0.0 47.0 %shard_map.73 = bf16[64,1024]{1,0:T(8,128)(2,1)} custom-call(bf16[64,1024]{1,0:T(8,128)(2,1)} %tok_hbm.1, f32[1,1024]{1,0:T(1,128)} %bitcast.3, s32[6,64]{1,0:T(8,128)} %bitcast.4, f32[6,64]{1,0:T(8,128)} %bitcast.5, bf16[1,1024,2048]{2,1,0:T(8,128)(2,1)} %wg_hbm.1, bf16[1,1024,2048]{2,1,0:T(8,128)(2,1)} %wu_hbm.1, bf16[1,2048,1024]{2,1,0:T(8,128)(2,1)} %wd_hbm.1), custom_call_target="tpu_custom_call" | custom-call | tf_op jit(solution)/shard_map/pallas_call | solution.py:330
  47.0 1.6 %copy.9 = bf16[64,1024]{1,0:T(8,128)(2,1)} copy(bf16[64,1024]{1,0:T(8,128)(2,1)} %shard_map.73) | data formatting | bytes 262144

commit v3 on v2

--- a/solution.py
+++ b/solution.py
@@ -58,7 +58,7 @@
 CORES = 2
 ROWS_Y = 2
 PLANE = CORES * ROWS_Y
-FF_TILE = 512
+FF_TILE = 2048
 HALVES = 2
 
 
@@ -291,14 +291,15 @@
             if last >= 2:
                 from_z(2)
             loads[2].wait()
-        if k >= 3:
-            z_stage(k - 2)
-        if k >= 1:
-            y_stage(k - 1)
+        if k == 1:
+            y_stage(0)
+        if k == last and k >= 2:
+            z_stage(k - 1)
         down(k)
-    if last >= 2:
-        z_stage(last - 1)
-    y_stage(last)
+        if k >= 1 or last == 0:
+            y_stage(k)
+        if 2 <= k < last:
+            z_stage(k - 1)
     totals = [layer_sum(0, h) for h in range(HALVES)]
     if last >= 1:
         z_stage(last)

time: 48.7 us -> 46.6 us (0.957)
  Pallas kernels: 47 us -> 44.8 us
    pallas_call x1, Pallas kernels: 47 us -> 44.8 us  [fused_shards(): pl.pallas_call(functools.partial(fused_kernel, layers, cap), out_shape=ja...]
where the time goes in v3:
time: 46.6 us; the launch traced here: 46.4 us
  Pallas kernels  44.8 us (96%)
  local copies, waits for them, and re-layouts  1.57 us (3%)
    pallas_call x1, Pallas kernels, fused_shards(): pl.pallas_call(functools.partial(fused_kernel, layers, cap), out_shape=ja...  44.8 us
    unnamed x1, local copies, waits for them, and re-layouts  1.57 us

profile of v3, /device:TPU:0, one launch (start us, length us, event | category | flops | bytes accessed | tf_op | source)
XLA Modules:
  0.0 46.4 jit_solution(4705199737946581832)
XLA Ops:
  0.0 44.8 %shard_map.73 = bf16[64,1024]{1,0:T(8,128)(2,1)} custom-call(bf16[64,1024]{1,0:T(8,128)(2,1)} %tok_hbm.1, f32[1,1024]{1,0:T(1,128)} %bitcast.3, s32[6,64]{1,0:T(8,128)} %bitcast.4, f32[6,64]{1,0:T(8,128)} %bitcast.5, bf16[1,1024,2048]{2,1,0:T(8,128)(2,1)} %wg_hbm.1, bf16[1,1024,2048]{2,1,0:T(8,128)(2,1)} %wu_hbm.1, bf16[1,2048,1024]{2,1,0:T(8,128)(2,1)} %wd_hbm.1), custom_call_target="tpu_custom_call" | custom-call | tf_op jit(solution)/shard_map/pallas_call | solution.py:331
  44.9 1.6 %copy.9 = bf16[64,1024]{1,0:T(8,128)(2,1)} copy(bf16[64,1024]{1,0:T(8,128)(2,1)} %shard_map.73) | data formatting | bytes 262144
